TPU v7x, 32 devices: a whole 2x2x4 slice. The times are simulated.
32 devices in a mesh: grp: 2 (over y), fs: 4 (over z), tp: 4 (over x, core).
Axes of the slice: x: 2, y: 2, z: 4, core: 2. Of those that a mesh axis runs over, the one named last changes fastest.
Arguments:
- tokens: bfloat16 [2048, 2048], P(('grp', 'fs', 'tp')), parts along dimension 0, may hold values from -30 to 30
- gate_master: float32 [2048, 2752], P('fs', 'tp'), may hold values from -0.125 to 0.125
- up_master: float32 [2048, 2752], P('fs', 'tp'), may hold values from -0.125 to 0.125
- down_master: float32 [2048, 2752], P('fs', 'tp'), may hold values from -0.4375 to 0.4375
- norm_gain: float32 [2048], replicated, may hold values from 0.1 to 1.9
- post_gain: float32 [2048], replicated, may hold values from 0.1 to 1.9
- post_bias: float32 [2048], replicated, may hold values from -3 to 3
Outputs:
- gate_ready: bfloat16 [4096, 2752], P('grp', 'tp'), parts along dimension 0
- up_ready: bfloat16 [4096, 2752], P('grp', 'tp'), parts along dimension 0
- down_ready: bfloat16 [4096, 2752], P('grp', 'tp'), parts along dimension 0
- result: bfloat16 [2048, 2048], P(('grp', 'fs', 'tp')), parts along dimension 0
There are 2 independent parts, one for each index of `grp`. A program takes and returns all parts, laid end to end along the dimension named above; an argument that names none is the same for every part. Nothing has to cross between parts.
All inputs are finite; a program needn't handle non-finite values.
Results may differ from a plain program's by a relative error of at most 0.009.
Values may be sent and summed in bfloat16 or wider, within the bound.
No kernel may reach another device: no remote copies, remote signals or barrier semaphores. Data moves between devices by JAX's collectives and lax.ppermute only.
A program may use at most 64 MiB of HBM per device.

v0:
```python
import functools

import jax
import jax.numpy as jnp
from jax import lax
from jax.experimental import pallas as pl
from jax.experimental.pallas import tpu as pltpu
from jax.sharding import PartitionSpec as P


BF16 = jnp.bfloat16
F32 = jnp.float32
ANY = pl.BlockSpec(memory_space=pl.ANY)
VMEM = pl.BlockSpec(memory_space=pltpu.VMEM)
LANES = 128
LONGEST_LINE = 8


def finish(wide, branch, post_gain, post_bias):
    mixed = jnp.sqrt(jnp.float32(2.0)) * wide + 0.5 * branch
    center = jnp.mean(mixed, axis=-1, keepdims=True)
    spread = jnp.mean(jnp.square(mixed - center), axis=-1, keepdims=True)
    return ((mixed - center) * lax.rsqrt(spread + 1e-05) * post_gain + post_bias).astype(
        jnp.bfloat16
    )


def plain(tokens, gate_master, up_master, down_master, norm_gain, post_gain, post_bias):
    row_count = gate_master.shape[0]
    first_row = lax.axis_index("fs") * row_count
    gain_rows = lax.dynamic_slice_in_dim(norm_gain, first_row, row_count, 0)
    gate_piece = (gain_rows[:, None] * gate_master).astype(BF16)
    up_piece = (gain_rows[:, None] * up_master).astype(BF16)
    down_piece = down_master.astype(BF16)
    gate_ready, up_ready, down_ready = (
        lax.all_gather(gate_piece, "fs", axis=0, tiled=True),
        lax.all_gather(up_piece, "fs", axis=0, tiled=True),
        lax.all_gather(down_piece, "fs", axis=0, tiled=True),
    )
    wide = tokens.astype(F32)
    normed = (wide * lax.rsqrt(jnp.mean(wide * wide, axis=-1, keepdims=True) + 1e-06)).astype(BF16)
    piece = lax.all_gather(normed, "tp", axis=0, tiled=True)
    gate = jnp.dot(piece, gate_ready, preferred_element_type=F32)
    upward = jnp.dot(piece, up_ready, preferred_element_type=F32)
    hidden = (jax.nn.silu(gate) * upward).astype(BF16)
    branch = lax.psum_scatter(
        lax.dot_general(
            hidden, down_ready, (((1,), (1,)), ((), ())), preferred_element_type=F32
        ).astype(BF16),
        "tp",
        scatter_dimension=0,
        tiled=True,
    ).astype(F32)
    return (gate_ready, up_ready, down_ready, finish(wide, branch, post_gain, post_bias))


class Line:
    def __init__(self, count):
        self.count = count
        self.swaps = []
        self.pairs = {}
        self.brings = {}
        for t in range(1, count):
            for q in (0, 1):
                pairs, brings = [], {}
                for i in range(q, count - 1, 2):
                    if i - t + 1 >= 0:
                        pairs.append((i, i + 1))
                        brings[i + 1] = i + 1 - t
                    if i + t < count:
                        pairs.append((i + 1, i))
                        brings[i] = i + t
                if pairs:
                    self.swaps.append((t, q))
                    self.pairs[t, q] = pairs
                    self.brings[t, q] = brings
        self.order = {f: [s for s in self.swaps if f in self.brings[s]] for f in range(count)}
        self.slots = [
            sorted({self.order[f][k] for f in range(count)}) for k in range(count - 1)
        ]

    def piece(self, f, k):
        out = jnp.int32(0)
        for i in range(self.count):
            s = self.order[i][k]
            out = jnp.where(f == i, jnp.int32(self.brings[s][i]), out)
        return out

    def holds(self, f, k, s):
        out = f < 0
        for i in range(self.count):
            if self.order[i][k] == s:
                out = jnp.logical_or(out, f == i)
        return out


MESH = ("grp", "fs", "tp")


def whole_moves(sizes, step):
    groups, n_fs, n_tok = (sizes[axis] for axis in MESH)

    def index(g, f, t):
        return (g * n_fs + f) * n_tok + t

    moves = []
    for g in range(groups):
        for f in range(n_fs):
            to = step(g, f)
            for t in range(n_tok):
                target = index(g, f, t ^ 1) if to is None else index(*to, t)
                moves.append((index(g, f, t), target))
    return moves


def line_exchange(line, halves, sizes):
    near, far = {}, {}
    for t, q in line.swaps:
        ends = {i for pair in line.pairs[t, q] for i in pair}

        def along(g, f):
            return (g, f + 1 if f % 2 == q else f - 1) if f in ends else None

        def across(g, f):
            return ((g + 1) % sizes["grp"], f) if f in line.brings[t, q] else None

        operand = halves[0] if t == 1 else near[t - 1, 1 - q]
        near[t, q] = lax.ppermute(operand, MESH, whole_moves(sizes, along))
        if t == 1 and len(halves) > 1:
            far[t, q] = lax.ppermute(halves[1], MESH, whole_moves(sizes, along))
        else:
            far[t, q] = lax.ppermute(near[t, q], MESH, whole_moves(sizes, across))
    return near, far


def at(start, size):
    return pl.ds(pl.multiple_of(start, LANES), size)


def cost(flops, moved):
    return pl.CostEstimate(flops=flops, bytes_accessed=moved, transcendentals=0)


def half_kernel(groups, cuts, *refs):
    *operands, buf, sem = refs
    master_ref, outs = operands[0], operands[-len(cuts):]
    whole = master_ref.shape[-1]
    width = outs[0].shape[-1]
    g, f = lax.axis_index("grp"), lax.axis_index("fs")
    starts = [(1 - g if side else g) * (whole // groups) + n * width for side, n in cuts]
    loads = [
        pltpu.make_async_copy(master_ref.at[:, at(start, width)], buf.at[n], sem.at[n])
        for n, start in enumerate(starts)
    ]
    for load in loads:
        load.start()
    for n, load in enumerate(loads):
        load.wait()
        value = buf[n]
        if len(operands) > len(cuts) + 1:
            value = value * operands[1][:, at(f * whole + starts[n], width)]
        outs[n][...] = value.astype(BF16)


def half_pieces(groups, width, cuts, master, gain=None):
    units = master.shape[0]
    count = len(cuts)
    operands = [master] if gain is None else [master, gain]
    return pl.pallas_call(
        functools.partial(half_kernel, groups, cuts),
        out_shape=(jax.ShapeDtypeStruct((units, width), BF16),) * count,
        in_specs=[ANY, VMEM][: len(operands)],
        out_specs=(VMEM,) * count,
        scratch_shapes=[
            pltpu.VMEM((count, units, width), F32),
            pltpu.SemaphoreType.DMA((count,)),
        ],
        cost_estimate=cost(2**32, 6 * units * width * count),
        compiler_params=pltpu.CompilerParams(vmem_limit_bytes=8 * 2**20),
        name="half_pieces",
    )(*operands)


def norm_kernel(tokens_ref, out_ref):
    wide = tokens_ref[...].astype(F32)
    scale = lax.rsqrt(jnp.mean(wide * wide, axis=-1, keepdims=True) + 1e-06)
    out_ref[...] = (wide * scale).astype(BF16)


def norm(tokens):
    return pl.pallas_call(
        norm_kernel,
        out_shape=jax.ShapeDtypeStruct(tokens.shape, BF16),
        in_specs=[VMEM],
        out_specs=VMEM,
        cost_estimate=cost(4 * tokens.size, 4 * tokens.size),
        compiler_params=pltpu.CompilerParams(vmem_limit_bytes=8 * 2**20),
        name="norm_tokens",
    )(tokens)


def slot_loads(line, f, k, refs, fill, sem):
    swaps = line.slots[k]

    def each(act):
        for s in swaps:
            if len(swaps) == 1:
                act(pltpu.make_async_copy(refs[s], fill, sem))
            else:

                @pl.when(line.holds(f, k, s))
                def _():
                    act(pltpu.make_async_copy(refs[s], fill, sem))

    return (lambda: each(lambda c: c.start())), (lambda: each(lambda c: c.wait()))


def taken(line, ks):
    return sorted({s for k in ks for s in line.slots[k]})


def split(refs, *counts):
    out = []
    for n in counts:
        out.append(refs[:n])
        refs = refs[n:]
    return (*out, refs)


def pair_kernel(line, ks, own, n_tok, *refs):
    swaps = taken(line, ks)
    toks, refs = split(refs, n_tok)
    tables = []
    for _ in range(4):
        some, refs = split(refs, len(swaps))
        tables.append(dict(zip(swaps, some)))
    if own:
        (gate_ref, up_ref, gain_ref), refs = split(refs, 3)
    else:
        (so_far, _, _), refs = split(refs, 3)
    gate_out, up_out, out_ref, normed, held, masters, sem_in, sem_m, sem_t, sem_out = refs
    g, f = lax.axis_index("grp"), lax.axis_index("fs")
    whole = toks[0].shape[-1] // line.count
    half = tables[0][swaps[0]].shape[-1]
    rows = toks[0].shape[0]
    first = 1 if own else 0
    places = ([f] if own else []) + [line.piece(f, k) for k in ks]
    mine = []
    if own:
        mine = [
            pltpu.make_async_copy(src, masters.at[n], sem_m.at[n])
            for n, src in enumerate((gate_ref, up_ref))
        ]
    for load in mine:
        load.start()
    loads = []
    for i, k in enumerate(ks):
        for n, table in enumerate(tables):
            h = 1 - g if n % 2 else g
            fill = held.at[n // 2, :, at((first + i) * whole + h * half, half)]
            loads.append(slot_loads(line, f, k, table, fill, sem_in.at[4 * i + n]))
    token_loads = [
        pltpu.make_async_copy(
            tok.at[:, at(place * whole, whole)],
            normed.at[pl.ds(d * rows, rows), pl.ds(i * whole, whole)],
            sem_t.at[d * len(places) + i],
        )
        for d, tok in enumerate(toks)
        for i, place in enumerate(places)
    ]
    for load in token_loads:
        load.start()
    for begin, _ in loads:
        begin()
    stores = [
        [
            pltpu.make_async_copy(
                held.at[n, :, pl.ds(i * whole, whole)],
                out.at[:, at(place * whole, whole)],
                sem_out.at[2 * i + n],
            )
            for n, out in enumerate((gate_out, up_out))
        ]
        for i, place in enumerate(places)
    ]
    if own:
        gain = gain_ref[:, at(f * whole, whole)]
        for n, load in enumerate(mine):
            load.wait()
            held[n, :, :whole] = (masters[n] * gain).astype(BF16)
            stores[0][n].start()
    for i in range(len(ks)):
        for _, end in loads[4 * i:4 * i + 4]:
            end()
        for store in stores[first + i]:
            store.start()
    for load in token_loads:
        load.wait()
    gate, up = [
        lax.dot_general(
            normed[...], held[n], (((1,), (1,)), ((), ())), preferred_element_type=F32
        )
        for n in range(2)
    ]
    if own:
        out_ref[0] = gate
        out_ref[1] = up
    else:
        gate = gate + so_far[0]
        up = up + so_far[1]
        out_ref[...] = (gate / (1.0 + jnp.exp(-gate)) * up).astype(BF16)
    for some in stores:
        for store in some:
            store.wait()


def pair_part(line, ks, toks, tables, masters, so_far):
    own = so_far is None
    rows, width = toks[0].shape
    whole = width // line.count
    n_tok = len(toks)
    swaps = taken(line, ks)
    units = tables[0][swaps[0]].shape[0]
    blocks = len(ks) + (1 if own else 0)
    operands = [*toks, *(table[s] for table in tables for s in swaps)]
    in_specs = [ANY] * len(operands)
    aliases = {}
    if own:
        operands += masters
        in_specs += [ANY, ANY, VMEM]
        last = jax.ShapeDtypeStruct((2, n_tok * rows, units), F32)
    else:
        aliases = {len(operands) + 1: 0, len(operands) + 2: 1}
        operands += so_far
        in_specs += [VMEM, ANY, ANY]
        last = jax.ShapeDtypeStruct((n_tok * rows, units), BF16)
    ready = jax.ShapeDtypeStruct((units, width), BF16)
    return pl.pallas_call(
        functools.partial(pair_kernel, line, ks, own, n_tok),
        out_shape=(ready, ready, last),
        in_specs=in_specs,
        out_specs=(ANY, ANY, VMEM),
        scratch_shapes=[
            pltpu.VMEM((n_tok * rows, blocks * whole), BF16),
            pltpu.VMEM((2, units, blocks * whole), BF16),
            pltpu.VMEM((2, units, whole), F32),
            pltpu.SemaphoreType.DMA((4 * len(ks),)),
            pltpu.SemaphoreType.DMA((2,)),
            pltpu.SemaphoreType.DMA((n_tok * blocks,)),
            pltpu.SemaphoreType.DMA((2 * blocks,)),
        ],
        input_output_aliases=aliases,
        cost_estimate=cost(4 * n_tok * rows * units * blocks * whole, 10 * units * blocks * whole),
        compiler_params=pltpu.CompilerParams(vmem_limit_bytes=24 * 2**20),
        name="pair_first" if own else "pair_last",
    )(*operands)


OWN = -1


class Blocks:
    def __init__(self, line, groups, whole, cut):
        self.line, self.groups, self.whole, self.cut = line, groups, whole, cut

    def width(self, block):
        return self.whole if block[0] == OWN else self.cut

    def widths(self, blocks):
        return sum(self.width(block) for block in blocks)

    def spans(self, blocks):
        n = 0
        for block in blocks:
            yield block, n, self.width(block)
            n += self.width(block)

    def column(self, block):
        g, f = lax.axis_index("grp"), lax.axis_index("fs")
        if block[0] == OWN:
            return f * self.whole
        k, side, n = block
        half = (1 - g if side else g) * (self.whole // self.groups)
        return self.line.piece(f, k) * self.whole + half + n * self.cut

    def sources(self, blocks):
        return sorted(
            {(b[1], b[2], s) for b in blocks if b[0] != OWN for s in self.line.slots[b[0]]}
        )

    def operands(self, blocks, tables):
        return [tables[n][side][s] for side, n, s in self.sources(blocks)]

    def loads(self, blocks, refs, held, sem):
        f = lax.axis_index("fs")
        named = dict(zip(self.sources(blocks), refs))
        waits = []
        for i, (block, start, width) in enumerate(self.spans(blocks)):
            if block[0] == OWN:
                continue
            k, side, n = block
            table = {s: named[side, n, s] for s in self.line.slots[k]}
            begin, end = slot_loads(
                self.line, f, k, table, held.at[:, pl.ds(start, width)], sem.at[i]
            )
            begin()
            waits.append(end)
        return waits

    def stores(self, blocks, held, out, sem):
        return [
            pltpu.make_async_copy(
                held.at[:, pl.ds(start, width)], out.at[:, at(self.column(block), width)], sem.at[i]
            )
            for i, (block, start, width) in enumerate(self.spans(blocks))
        ]


def multiply(hidden_ref, held, start, stop, parts):
    rows = parts[0].shape[0]
    part = jnp.dot(
        hidden_ref[...], held[:, start:stop], preferred_element_type=F32
    ).astype(BF16)
    for d, ref in enumerate(parts):
        ref[:, start:stop] = part[d * rows:(d + 1) * rows]


def down_own_kernel(form, blocks, n_tok, *refs):
    count = len(form.sources(blocks))
    (hidden_ref, master), some, (down_out,), parts, scratch = split(refs, 2, count, 1, n_tok)
    held, wide, sem_in, sem_m, sem_out = scratch
    mine = pltpu.make_async_copy(master, wide, sem_m)
    mine.start()
    waits = form.loads(blocks, some, held, sem_in)
    first, *others = form.stores(blocks, held, down_out, sem_out)
    mine.wait()
    held[:, :form.whole] = wide[...].astype(BF16)
    first.start()
    multiply(hidden_ref, held, 0, form.whole, parts)
    for wait in waits:
        wait()
    for store in others:
        store.start()
    multiply(hidden_ref, held, form.whole, form.widths(blocks), parts)
    for store in (first, *others):
        store.wait()


def down_own(form, blocks, n_tok, hidden, tables, master):
    some = form.operands(blocks, tables)
    units = master.shape[0]
    rows = hidden.shape[0] // n_tok
    width = form.widths(blocks)
    return pl.pallas_call(
        functools.partial(down_own_kernel, form, blocks, n_tok),
        out_shape=(jax.ShapeDtypeStruct((units, form.whole * form.line.count), BF16),)
        + (jax.ShapeDtypeStruct((rows, width), BF16),) * n_tok,
        in_specs=[VMEM] + [ANY] * (len(some) + 1),
        out_specs=(ANY,) + (VMEM,) * n_tok,
        scratch_shapes=[
            pltpu.VMEM((units, width), BF16),
            pltpu.VMEM((units, form.whole), F32),
            pltpu.SemaphoreType.DMA((len(blocks),)),
            pltpu.SemaphoreType.DMA,
            pltpu.SemaphoreType.DMA((len(blocks),)),
        ],
        cost_estimate=cost(2 * hidden.size * width, 4 * units * width),
        compiler_params=pltpu.CompilerParams(vmem_limit_bytes=12 * 2**20),
        name="down_own",
    )(hidden, master, *some)


def down_more_kernel(form, blocks, n_tok, *refs):
    (hidden_ref,), some, parts, (held, sem_in) = split(refs, 1, len(form.sources(blocks)), n_tok)
    for wait in form.loads(blocks, some, held, sem_in):
        wait()
    multiply(hidden_ref, held, 0, form.widths(blocks), parts)


def down_more(form, blocks, n_tok, hidden, tables):
    some = form.operands(blocks, tables)
    units = hidden.shape[1]
    rows = hidden.shape[0] // n_tok
    width = form.widths(blocks)
    return pl.pallas_call(
        functools.partial(down_more_kernel, form, blocks, n_tok),
        out_shape=(jax.ShapeDtypeStruct((rows, width), BF16),) * n_tok,
        in_specs=[VMEM] + [ANY] * len(some),
        out_specs=(VMEM,) * n_tok,
        scratch_shapes=[
            pltpu.VMEM((units, width), BF16),
            pltpu.SemaphoreType.DMA((len(blocks),)),
        ],
        cost_estimate=cost(2 * hidden.size * width, 2 * units * width),
        compiler_params=pltpu.CompilerParams(vmem_limit_bytes=8 * 2**20),
        name="down_more",
    )(hidden, *some)


def place_kernel(form, blocks, *refs):
    (_,), some, (down_out, held, sem_in, sem_out) = split(refs, 1, len(form.sources(blocks)))
    waits = form.loads(blocks, some, held, sem_in)
    stores = form.stores(blocks, held, down_out, sem_out)
    for wait, store in zip(waits, stores):
        wait()
        store.start()
    for store in stores:
        store.wait()


def place(form, blocks, ready, tables):
    some = form.operands(blocks, tables)
    units = ready.shape[0]
    width = form.widths(blocks)
    return pl.pallas_call(
        functools.partial(place_kernel, form, blocks),
        out_shape=jax.ShapeDtypeStruct(ready.shape, ready.dtype),
        in_specs=[ANY] * (len(some) + 1),
        out_specs=ANY,
        scratch_shapes=[
            pltpu.VMEM((units, width), BF16),
            pltpu.SemaphoreType.DMA((len(blocks),)),
            pltpu.SemaphoreType.DMA((len(blocks),)),
        ],
        input_output_aliases={0: 0},
        cost_estimate=cost(0, 4 * units * width),
        compiler_params=pltpu.CompilerParams(vmem_limit_bytes=8 * 2**20),
        name="place",
    )(ready, *some)


def mixed_blocks(form, blocks, tokens_ref, bufs):
    out = []
    for block, start, width in form.spans(blocks):
        cols = at(form.column(block), width)
        total = sum(buf[:, start:start + width].astype(F32) for buf in bufs)
        wide = tokens_ref[:, cols].astype(F32)
        out.append((cols, jnp.sqrt(F32(2.0)) * wide + 0.5 * total))
    return out


def mix_kernel(form, parts, n_tok, *refs):
    tokens_ref, *bufs, out_ref = refs
    n = 0
    for p, blocks in enumerate(parts):
        some = bufs[p * n_tok:(p + 1) * n_tok]
        for _, value in mixed_blocks(form, blocks, tokens_ref, some):
            out_ref[:, n:n + value.shape[1]] = value
            n += value.shape[1]


def mix(form, parts, tokens, values):
    flat = [x for some in values for x in some]
    width = sum(form.widths(blocks) for blocks in parts)
    return pl.pallas_call(
        functools.partial(mix_kernel, form, parts, len(values[0])),
        out_shape=jax.ShapeDtypeStruct((tokens.shape[0], width), F32),
        in_specs=[VMEM] * (1 + len(flat)),
        out_specs=VMEM,
        cost_estimate=cost(8 * tokens.shape[0] * width, 12 * tokens.shape[0] * width),
        compiler_params=pltpu.CompilerParams(vmem_limit_bytes=8 * 2**20),
        name="mix",
    )(tokens, *flat)


def finish_kernel(form, soon, late, *refs):
    tokens_ref, gain_ref, bias_ref, head_ref, *bufs, out_ref = refs
    width = tokens_ref.shape[-1]
    mixed = [
        (at(form.column(block), size), head_ref[:, start:start + size])
        for block, start, size in form.spans(soon)
    ]
    mixed += mixed_blocks(form, late, tokens_ref, bufs)
    center = sum(jnp.sum(m, axis=-1, keepdims=True) for _, m in mixed) / width
    spread = sum(jnp.sum(jnp.square(m - center), axis=-1, keepdims=True) for _, m in mixed) / width
    scale = lax.rsqrt(spread + 1e-05)
    for cols, m in mixed:
        out_ref[:, cols] = ((m - center) * scale * gain_ref[:, cols] + bias_ref[:, cols]).astype(BF16)


def finish_all(form, soon, late, tokens, gain, bias, head, parts):
    return pl.pallas_call(
        functools.partial(finish_kernel, form, soon, late),
        out_shape=jax.ShapeDtypeStruct(tokens.shape, BF16),
        in_specs=[VMEM] * (4 + len(parts)),
        out_specs=VMEM,
        cost_estimate=cost(16 * tokens.size, 16 * tokens.size),
        compiler_params=pltpu.CompilerParams(vmem_limit_bytes=8 * 2**20),
        name="finish",
    )(tokens, gain, bias, head, *parts)


def over_tp(blocks, n_tok):
    return [blocks[0]] + [
        lax.ppermute(blocks[d], "tp", [(i, i ^ d) for i in range(n_tok)])
        for d in range(1, n_tok)
    ]


def exchanged(sizes, tokens, gate_master, up_master, down_master, norm_gain, post_gain, post_bias):
    groups, n_tok = sizes["grp"], sizes["tp"]
    line = Line(sizes["fs"])
    gate, up, down = gate_master.T, up_master.T, down_master.T
    gain = norm_gain[None, :]
    last = line.count - 2
    most = tuple(range(last))

    whole = down.shape[1]
    half, cut = whole // groups, whole // groups // 2
    mine, other = 0, 1

    tables = {}
    for tag, width, cuts, *operands in (
        ("d", cut, ((mine, 0),), down),
        ("g", half, ((mine, 0),), gate, gain),
        ("u", half, ((mine, 0),), up, gain),
        ("e", cut, ((mine, 1), (other, 1)), down),
    ):
        halves = half_pieces(groups, width, cuts, *operands)
        tables[tag] = line_exchange(line, halves, sizes)
    pair_tables = (*tables["g"], *tables["u"])
    toks = over_tp([norm(tokens)] * n_tok, n_tok)
    gate_ready, up_ready, so_far = pair_part(line, most, toks, pair_tables, [gate, up, gain], None)
    gate_ready, up_ready, hidden = pair_part(
        line, (last,), toks, pair_tables, None,
        [so_far, gate_ready, up_ready],
    )
    form = Blocks(line, groups, whole, cut)
    down_tables = (tables["d"], tables["e"])
    early = ((OWN,), (0, mine, 0), (0, other, 0), *((k, mine, 0) for k in most[1:]), (0, mine, 1))
    late = ((0, other, 1), (last, other, 1))
    between = tuple(
        block
        for block in ((k, s, n) for n in (0, 1) for k in range(last + 1) for s in (mine, other))
        if block not in early and block not in late
    )
    down_ready, *own = down_own(form, early, n_tok, hidden, down_tables, down)
    own = over_tp(own, n_tok)
    rest = down_more(form, between, n_tok, hidden, down_tables)
    rest = over_tp(rest, n_tok)
    end = down_more(form, late, n_tok, hidden, down_tables)
    end = over_tp(end, n_tok)
    down_ready = place(form, between + late, down_ready, down_tables)
    head = mix(form, (early, between), tokens, (own, rest))
    result = finish_all(
        form, early + between, late, tokens,
        post_gain[None, :], post_bias[None, :], head, end,
    )
    return (gate_ready.T, up_ready.T, down_ready.T, result)


def fits(sizes, tokens, gate_master):
    groups, n_fs, n_tok = sizes["grp"], sizes["fs"], sizes["tp"]
    rows = gate_master.shape[0] // n_fs
    units = gate_master.shape[1] // n_tok
    return (
        groups == 2
        and 2 < n_fs <= LONGEST_LINE
        and n_tok > 1
        and n_tok & (n_tok - 1) == 0
        and rows % (groups * 2 * LANES) == 0
        and units % 16 == 0
        and tokens.shape[0] // (groups * n_fs * n_tok) % 16 == 0
    )


def solution(mesh):
    sizes = dict(mesh.shape)
    rows = P(("grp", "fs", "tp"), None)
    ready = P("grp", "tp")

    def over_mesh(body):
        return jax.shard_map(
            body,
            mesh=mesh,
            in_specs=(rows, P("fs", "tp"), P("fs", "tp"), P("fs", "tp"), P(), P(), P()),
            out_specs=(ready, ready, ready, rows),
            check_vma=False,
        )

    def run(tokens, gate_master, *rest):
        if not fits(sizes, tokens, gate_master):
            return over_mesh(plain)(tokens, gate_master, *rest)
        step = over_mesh(functools.partial(exchanged, sizes))
        return step(tokens, gate_master, *rest)

    return run
```

profile of v0, /device:TPU:0, one launch (start us, length us, event | category | flops | bytes accessed | tf_op | source)
XLA Modules:
  0.0 148.5 jit_solution(16488922802754406438)
XLA Ops:
  2.2 3.1 %collective-permute-start.26 = (bf16[688,128]{1,0:T(8,128)(2,1)S(1)}, bf16[688,128]{1,0:T(8,128)(2,1)S(1)}, u32[]{:S(2)}, u32[]{:S(2)}) collective-permute-start(bf16[688,128]{1,0:T(8,128)(2,1)S(1)} %get-tuple-element.31), channel_id=1, source_target_pairs={{0,4},{1,5},{2,6},{3,7},{4,0},{5,1},{6,2},{7,3},{8,12},{9,13},{10,... | collective-permute-start | bytes 528392 | tf_op jit(solution)/shard_map/ppermute | solution.py:128
  5.4 3.2 %collective-permute-start.23 = (bf16[688,128]{1,0:T(8,128)(2,1)S(1)}, bf16[688,128]{1,0:T(8,128)(2,1)S(1)}, u32[]{:S(2)}, u32[]{:S(2)}) collective-permute-start(bf16[688,128]{1,0:T(8,128)(2,1)S(1)} %half_pieces.6), channel_id=1, source_target_pairs={{0,4},{1,5},{2,6},{3,7},{4,0},{5,1},{6,2},{7,3},{8,12},{9,13},{10,... | collective-permute-start | bytes 528392 | tf_op jit(solution)/shard_map/ppermute | solution.py:128
  9.5 4.0 %collective-permute-done.23.refs_2_ = bf16[688,128]{1,0:T(8,128)(2,1)S(1)} collective-permute-done((bf16[688,128]{1,0:T(8,128)(2,1)S(1)}, bf16[688,128]{1,0:T(8,128)(2,1)S(1)}, u32[]{:S(2)}, u32[]{:S(2)}) %collective-permute-start.23) | collective-permute-done | bytes 176160 | tf_op jit(solution)/shard_map/ppermute | solution.py:128
  17.6 15.3 %collective-permute-start.3 = (bf16[688,256]{1,0:T(8,128)(2,1)S(1)}, bf16[688,256]{1,0:T(8,128)(2,1)S(1)}, u32[]{:S(2)}, u32[]{:S(2)}) collective-permute-start(bf16[688,256]{1,0:T(8,128)(2,1)S(1)} %half_pieces.4), channel_id=1, source_target_pairs={{0,4},{1,5},{2,6},{3,7},{4,0},{5,1},{6,2},{7,3},{8,12},{9,13},{10,... | collective-permute-start | bytes 1056776 | tf_op jit(solution)/shard_map/ppermute | solution.py:128
  33.5 8.9 %collective-permute-start.31 = (bf16[688,128]{1,0:T(8,128)(2,1)S(1)}, bf16[688,128]{1,0:T(8,128)(2,1)S(1)}, u32[]{:S(2)}, u32[]{:S(2)}) collective-permute-start(bf16[688,128]{1,0:T(8,128)(2,1)S(1)} %collective-permute-done.30.refs_3_), channel_id=1, source_target_pairs={{0,4},{1,5},{2,6},{3,7},{4,0},{5,1},{6,2},{7,3},{8,12},{9,13},{10,... | collective-permute-start | bytes 528392 | tf_op jit(solution)/shard_map/ppermute | solution.py:128
  44.0 5.5 %collective-permute-done.8.refs_10_ = bf16[688,256]{1,0:T(8,128)(2,1)S(1)} collective-permute-done((bf16[688,256]{1,0:T(8,128)(2,1)S(1)}, bf16[688,256]{1,0:T(8,128)(2,1)S(1)}, u32[]{:S(2)}, u32[]{:S(2)}) %collective-permute-start.8) | collective-permute-done | bytes 352288 | tf_op jit(solution)/shard_map/ppermute | solution.py:128
  49.6 3.5 %collective-permute-start.29 = (bf16[688,128]{1,0:T(8,128)(2,1)S(1)}, bf16[688,128]{1,0:T(8,128)(2,1)S(1)}, u32[]{:S(2)}, u32[]{:S(2)}) collective-permute-start(bf16[688,128]{1,0:T(8,128)(2,1)S(1)} %collective-permute-done.28.refs_1_), channel_id=1, source_target_pairs={{0,4},{1,5},{2,6},{3,7},{4,0},{5,1},{6,2},{7,3},{8,12},{9,13},{10,... | collective-permute-start | bytes 528392 | tf_op jit(solution)/shard_map/ppermute | solution.py:128
  53.3 2.0 %collective-permute-start.33 = (bf16[688,128]{1,0:T(8,128)(2,1)S(1)}, bf16[688,128]{1,0:T(8,128)(2,1)S(1)}, u32[]{:S(2)}, u32[]{:S(2)}) collective-permute-start(bf16[688,128]{1,0:T(8,128)(2,1)S(1)} %collective-permute-done.32.refs_5_), channel_id=1, source_target_pairs={{0,4},{1,5},{2,6},{3,7},{4,0},{5,1},{6,2},{7,3},{8,12},{9,13},{10,... | collective-permute-start | bytes 528392 | tf_op jit(solution)/shard_map/ppermute | solution.py:128
  55.4 1.8 %collective-permute-done.25.refs_4_ = bf16[688,128]{1,0:T(8,128)(2,1)S(1)} collective-permute-done((bf16[688,128]{1,0:T(8,128)(2,1)S(1)}, bf16[688,128]{1,0:T(8,128)(2,1)S(1)}, u32[]{:S(2)}, u32[]{:S(2)}) %collective-permute-start.25) | collective-permute-done | bytes 176160 | tf_op jit(solution)/shard_map/ppermute | solution.py:128
  58.6 2.2 %collective-permute-done.29.refs_2_ = bf16[688,128]{1,0:T(8,128)(2,1)S(1)} collective-permute-done((bf16[688,128]{1,0:T(8,128)(2,1)S(1)}, bf16[688,128]{1,0:T(8,128)(2,1)S(1)}, u32[]{:S(2)}, u32[]{:S(2)}) %collective-permute-start.29) | collective-permute-done | bytes 176160 | tf_op jit(solution)/shard_map/ppermute | solution.py:128
  62.4 8.6 %collective-permute-done.33.refs_6_ = bf16[688,128]{1,0:T(8,128)(2,1)S(1)} collective-permute-done((bf16[688,128]{1,0:T(8,128)(2,1)S(1)}, bf16[688,128]{1,0:T(8,128)(2,1)S(1)}, u32[]{:S(2)}, u32[]{:S(2)}) %collective-permute-start.33) | collective-permute-done | bytes 176160 | tf_op jit(solution)/shard_map/ppermute | solution.py:128
  71.0 1.7 %collective-permute-start.19 = (bf16[688,256]{1,0:T(8,128)(2,1)S(1)}, bf16[688,256]{1,0:T(8,128)(2,1)S(1)}, u32[]{:S(2)}, u32[]{:S(2)}) collective-permute-start(bf16[688,256]{1,0:T(8,128)(2,1)S(1)} %collective-permute-done.18.refs_11_), channel_id=1, source_target_pairs={{0,4},{1,5},{2,6},{3,7},{4,0},{5,1},{6,2},{7,3},{8,12},{9,13},{10,... | collective-permute-start | bytes 1056776 | tf_op jit(solution)/shard_map/ppermute | solution.py:128
  74.8 5.2 %collective-permute-done.19.refs_12_ = bf16[688,256]{1,0:T(8,128)(2,1)S(1)} collective-permute-done((bf16[688,256]{1,0:T(8,128)(2,1)S(1)}, bf16[688,256]{1,0:T(8,128)(2,1)S(1)}, u32[]{:S(2)}, u32[]{:S(2)}) %collective-permute-start.19) | collective-permute-done | bytes 352288 | tf_op jit(solution)/shard_map/ppermute | solution.py:128
  83.3 8.4 %collective-permute-start.10 = (bf16[688,256]{1,0:T(8,128)(2,1)S(1)}, bf16[688,256]{1,0:T(8,128)(2,1)S(1)}, u32[]{:S(2)}, u32[]{:S(2)}) collective-permute-start(bf16[688,256]{1,0:T(8,128)(2,1)S(1)} %collective-permute-done.9.refs_8_), channel_id=1, source_target_pairs={{0,4},{1,5},{2,6},{3,7},{4,0},{5,1},{6,2},{7,3},{8,12},{9,13},{10,... | collective-permute-start | bytes 1056776 | tf_op jit(solution)/shard_map/ppermute | solution.py:128
  93.3 4.7 %collective-permute-done.17.refs_9_ = bf16[688,256]{1,0:T(8,128)(2,1)S(1)} collective-permute-done((bf16[688,256]{1,0:T(8,128)(2,1)S(1)}, bf16[688,256]{1,0:T(8,128)(2,1)S(1)}, u32[]{:S(2)}, u32[]{:S(2)}) %collective-permute-start.17) | collective-permute-done | bytes 352288 | tf_op jit(solution)/shard_map/ppermute | solution.py:132
  98.0 2.8 %collective-permute-done.10.refs_9_ = bf16[688,256]{1,0:T(8,128)(2,1)S(1)} collective-permute-done((bf16[688,256]{1,0:T(8,128)(2,1)S(1)}, bf16[688,256]{1,0:T(8,128)(2,1)S(1)}, u32[]{:S(2)}, u32[]{:S(2)}) %collective-permute-start.10) | collective-permute-done | bytes 352288 | tf_op jit(solution)/shard_map/ppermute | solution.py:128
  102.3 5.8 %collective-permute-done.5.refs_5_ = bf16[688,256]{1,0:T(8,128)(2,1)S(1)} collective-permute-done((bf16[688,256]{1,0:T(8,128)(2,1)S(1)}, bf16[688,256]{1,0:T(8,128)(2,1)S(1)}, u32[]{:S(2)}, u32[]{:S(2)}) %collective-permute-start.5) | collective-permute-done | bytes 352288 | tf_op jit(solution)/shard_map/ppermute | solution.py:128
  110.1 5.3 %collective-permute-start.38 = (bf16[688,128]{1,0:T(8,128)(2,1)S(1)}, bf16[688,128]{1,0:T(8,128)(2,1)S(1)}, u32[]{:S(2)}, u32[]{:S(2)}) collective-permute-start(bf16[688,128]{1,0:T(8,128)(2,1)S(1)} %get-tuple-element.33), channel_id=1, source_target_pairs={{0,4},{1,5},{2,6},{3,7},{4,0},{5,1},{6,2},{7,3},{8,12},{9,13},{10,... | collective-permute-start | bytes 528392 | tf_op jit(solution)/shard_map/ppermute | solution.py:130
  117.0 2.6 %collective-permute-done.7.refs_7_ = bf16[688,256]{1,0:T(8,128)(2,1)S(1)} collective-permute-done((bf16[688,256]{1,0:T(8,128)(2,1)S(1)}, bf16[688,256]{1,0:T(8,128)(2,1)S(1)}, u32[]{:S(2)}, u32[]{:S(2)}) %collective-permute-start.7) | collective-permute-done | bytes 352288 | tf_op jit(solution)/shard_map/ppermute | solution.py:132
  121.1 3.2 %pair_first.1 = (bf16[688,2048]{1,0:T(8,128)(2,1)}, bf16[688,2048]{1,0:T(8,128)(2,1)}, f32[2,256,688]{2,1,0:T(8,128)S(1)}) custom-call(bf16[64,2048]{1,0:T(8,128)(2,1)S(1)} %norm_tokens.1.refs_0_, bf16[64,2048]{1,0:T(8,128)(2,1)S(1)} %collective-permute-done.refs_1_, bf16[64,2048]{1,0:T(8,128)(2,1)S(1)} %collective-permute-done.1.refs_2_, ...), custom_call_target="tpu_custom_call" | custom-call | flops 1082130432 | bytes 10567680 | tf_op jit(solution)/shard_map/pair_first/pallas_call | solution.py:338
  127.2 1.7 %down_own.1 = (bf16[688,2048]{1,0:T(8,128)(2,1)}, bf16[64,1024]{1,0:T(8,128)(2,1)S(1)}, bf16[64,1024]{1,0:T(8,128)(2,1)S(1)}, bf16[64,1024]{1,0:T(8,128)(2,1)S(1)}, bf16[64,1024]{1,0:T(8,128)(2,1)S(1)}) custom-call(bf16[256,688]{1,0:T(8,128)(2,1)S(1)} %get-tuple-element.30.refs_0_, f32[688,512]{1,0:T(8,128)S(1)} %bitcast.11, ...), custom_call_target="tpu_custom_call" | custom-call | flops 360710144 | bytes 2818048 | tf_op jit(solution)/shard_map/down_own/pallas_call | solution.py:454
  129.0 2.6 %collective-permute-start.47 = (bf16[64,768]{1,0:T(8,128)(2,1)S(1)}, bf16[64,768]{1,0:T(8,128)(2,1)S(1)}, u32[]{:S(2)}, u32[]{:S(2)}) collective-permute-start(bf16[64,768]{1,0:T(8,128)(2,1)S(1)} %get-tuple-element.40), channel_id=1, source_target_pairs={{0,2},{1,3},{2,0},{3,1},{4,6},{5,7},{6,4},{7,5},{8,10},{9,11},{10,... | collective-permute-start | bytes 294920 | tf_op jit(solution)/shard_map/ppermute | solution.py:595
  135.2 7.2 %collective-permute-done.48.refs_8_ = bf16[64,768]{1,0:T(8,128)(2,1)S(1)} collective-permute-done((bf16[64,768]{1,0:T(8,128)(2,1)S(1)}, bf16[64,768]{1,0:T(8,128)(2,1)S(1)}, u32[]{:S(2)}, u32[]{:S(2)}) %collective-permute-start.48) | collective-permute-done | bytes 98336 | tf_op jit(solution)/shard_map/ppermute | solution.py:595
  143.9 1.7 %place.1 = bf16[688,2048]{1,0:T(8,128)(2,1)} custom-call(bf16[688,2048]{1,0:T(8,128)(2,1)} %get-tuple-element.32.refs_0_, bf16[688,128]{1,0:T(8,128)(2,1)S(1)} %collective-permute-done.28.refs_1_, bf16[688,128]{1,0:T(8,128)(2,1)S(1)} %collective-permute-done.29.refs_2_, ...), custom_call_target="tpu_custom_call", output_to_operand_aliasing={{}: (0, {})} | custom-call | bytes 2818048 | tf_op jit(solution)/shard_map/place/pallas_call | solution.py:515
  (109 shorter events, 36.4 us)
Async XLA Ops:
  13.5 19.4 %collective-permute-start.1 = (bf16[64,2048]{1,0:T(8,128)(2,1)S(1)}, bf16[64,2048]{1,0:T(8,128)(2,1)S(1)}, u32[]{:S(2)}, u32[]{:S(2)}) collective-permute-start(bf16[64,2048]{1,0:T(8,128)(2,1)S(1)} %norm_tokens.1.refs_0_), channel_id=1, source_target_pairs={{0,2},{1,3},{2,0},{3,1},{4,6},{5,7},{6,4},{7,5},{8,10},{9,11},{10,... | collective-permute-start | bytes 786440 | tf_op jit(solution)/shard_map/ppermute | solution.py:595
  15.2 17.8 %collective-permute-start.2 = (bf16[64,2048]{1,0:T(8,128)(2,1)S(1)}, bf16[64,2048]{1,0:T(8,128)(2,1)S(1)}, u32[]{:S(2)}, u32[]{:S(2)}) collective-permute-start(bf16[64,2048]{1,0:T(8,128)(2,1)S(1)} %norm_tokens.1.refs_0_), channel_id=1, source_target_pairs={{0,3},{1,2},{2,1},{3,0},{4,7},{5,6},{6,5},{7,4},{8,11},{9,10},{10,... | collective-permute-start | bytes 786440 | tf_op jit(solution)/shard_map/ppermute | solution.py:595
  15.2 17.8 %collective-permute-start.13 = (bf16[688,256]{1,0:T(8,128)(2,1)S(1)}, bf16[688,256]{1,0:T(8,128)(2,1)S(1)}, u32[]{:S(2)}, u32[]{:S(2)}) collective-permute-start(bf16[688,256]{1,0:T(8,128)(2,1)S(1)} %half_pieces.4), channel_id=1, source_target_pairs={{0,1},{1,0},{2,3},{3,2},{4,8},{5,9},{6,10},{7,11},{8,4},{9,5},{10,... | collective-permute-start | bytes 1056776 | tf_op jit(solution)/shard_map/ppermute | solution.py:128
  17.2 16.3 %collective-permute-start.18 = (bf16[688,256]{1,0:T(8,128)(2,1)S(1)}, bf16[688,256]{1,0:T(8,128)(2,1)S(1)}, u32[]{:S(2)}, u32[]{:S(2)}) collective-permute-start(bf16[688,256]{1,0:T(8,128)(2,1)S(1)} %half_pieces.5), channel_id=1, source_target_pairs={{0,1},{1,0},{2,3},{3,2},{4,8},{5,9},{6,10},{7,11},{8,4},{9,5},{10,... | collective-permute-start | bytes 1056776 | tf_op jit(solution)/shard_map/ppermute | solution.py:128
  17.6 24.8 %collective-permute-start.3 = (bf16[688,256]{1,0:T(8,128)(2,1)S(1)}, bf16[688,256]{1,0:T(8,128)(2,1)S(1)}, u32[]{:S(2)}, u32[]{:S(2)}) collective-permute-start(bf16[688,256]{1,0:T(8,128)(2,1)S(1)} %half_pieces.4), channel_id=1, source_target_pairs={{0,4},{1,5},{2,6},{3,7},{4,0},{5,1},{6,2},{7,3},{8,12},{9,13},{10,... | collective-permute-start | bytes 1056776 | tf_op jit(solution)/shard_map/ppermute | solution.py:128
  32.9 16.6 %collective-permute-start.8 = (bf16[688,256]{1,0:T(8,128)(2,1)S(1)}, bf16[688,256]{1,0:T(8,128)(2,1)S(1)}, u32[]{:S(2)}, u32[]{:S(2)}) collective-permute-start(bf16[688,256]{1,0:T(8,128)(2,1)S(1)} %half_pieces.5), channel_id=1, source_target_pairs={{0,4},{1,5},{2,6},{3,7},{4,0},{5,1},{6,2},{7,3},{8,12},{9,13},{10,... | collective-permute-start | bytes 1056776 | tf_op jit(solution)/shard_map/ppermute | solution.py:128
  33.0 16.6 %collective-permute-start.28 = (bf16[688,128]{1,0:T(8,128)(2,1)S(1)}, bf16[688,128]{1,0:T(8,128)(2,1)S(1)}, u32[]{:S(2)}, u32[]{:S(2)}) collective-permute-start(bf16[688,128]{1,0:T(8,128)(2,1)S(1)} %collective-permute-done.23.refs_2_), channel_id=1, source_target_pairs={{0,1},{1,0},{2,3},{3,2},{4,8},{5,9},{6,10},{7,11},{8,4},{9,5},{10,... | collective-permute-start | bytes 528392 | tf_op jit(solution)/shard_map/ppermute | solution.py:128
  33.0 20.1 %collective-permute-start.32 = (bf16[688,128]{1,0:T(8,128)(2,1)S(1)}, bf16[688,128]{1,0:T(8,128)(2,1)S(1)}, u32[]{:S(2)}, u32[]{:S(2)}) collective-permute-start(bf16[688,128]{1,0:T(8,128)(2,1)S(1)} %collective-permute-done.26.refs_5_), channel_id=1, source_target_pairs={{0,1},{1,0},{2,3},{3,2},{4,8},{5,9},{6,10},{7,11},{8,4},{9,5},{10,... | collective-permute-start | bytes 528392 | tf_op jit(solution)/shard_map/ppermute | solution.py:128
  33.5 19.8 %collective-permute-start.31 = (bf16[688,128]{1,0:T(8,128)(2,1)S(1)}, bf16[688,128]{1,0:T(8,128)(2,1)S(1)}, u32[]{:S(2)}, u32[]{:S(2)}) collective-permute-start(bf16[688,128]{1,0:T(8,128)(2,1)S(1)} %collective-permute-done.30.refs_3_), channel_id=1, source_target_pairs={{0,4},{1,5},{2,6},{3,7},{4,0},{5,1},{6,2},{7,3},{8,12},{9,13},{10,... | collective-permute-start | bytes 528392 | tf_op jit(solution)/shard_map/ppermute | solution.py:128
  53.1 21.6 %collective-permute-start.14 = (bf16[688,256]{1,0:T(8,128)(2,1)S(1)}, bf16[688,256]{1,0:T(8,128)(2,1)S(1)}, u32[]{:S(2)}, u32[]{:S(2)}) collective-permute-start(bf16[688,256]{1,0:T(8,128)(2,1)S(1)} %collective-permute-done.13.refs_5_), channel_id=1, source_target_pairs={{0,4},{1,5},{2,6},{3,7},{4,0},{5,1},{6,2},{7,3},{8,12},{9,13},{10,... | collective-permute-start | bytes 1056776 | tf_op jit(solution)/shard_map/ppermute | solution.py:128
  53.3 17.6 %collective-permute-start.33 = (bf16[688,128]{1,0:T(8,128)(2,1)S(1)}, bf16[688,128]{1,0:T(8,128)(2,1)S(1)}, u32[]{:S(2)}, u32[]{:S(2)}) collective-permute-start(bf16[688,128]{1,0:T(8,128)(2,1)S(1)} %collective-permute-done.32.refs_5_), channel_id=1, source_target_pairs={{0,4},{1,5},{2,6},{3,7},{4,0},{5,1},{6,2},{7,3},{8,12},{9,13},{10,... | collective-permute-start | bytes 528392 | tf_op jit(solution)/shard_map/ppermute | solution.py:128
  57.1 15.6 %collective-permute-start.40 = (bf16[688,128]{1,0:T(8,128)(2,1)S(1)}, bf16[688,128]{1,0:T(8,128)(2,1)S(1)}, u32[]{:S(2)}, u32[]{:S(2)}) collective-permute-start(bf16[688,128]{1,0:T(8,128)(2,1)S(1)} %collective-permute-done.31.refs_4_), channel_id=1, source_target_pairs={{0,16},{1,17},{2,18},{3,19},{4,5},{5,4},{6,7},{7,6},{8,9},{9,8},{1... | collective-permute-start | bytes 528392 | tf_op jit(solution)/shard_map/ppermute | solution.py:132
  58.6 15.6 %collective-permute-start.36 = (bf16[688,128]{1,0:T(8,128)(2,1)S(1)}, bf16[688,128]{1,0:T(8,128)(2,1)S(1)}, u32[]{:S(2)}, u32[]{:S(2)}) collective-permute-start(bf16[688,128]{1,0:T(8,128)(2,1)S(1)} %collective-permute-done.28.refs_1_), channel_id=1, source_target_pairs={{0,1},{1,0},{2,3},{3,2},{4,20},{5,21},{6,22},{7,23},{8,24},{9,25},... | collective-permute-start | bytes 528392 | tf_op jit(solution)/shard_map/ppermute | solution.py:132
  74.7 16.9 %collective-permute-start.4 = (bf16[688,256]{1,0:T(8,128)(2,1)S(1)}, bf16[688,256]{1,0:T(8,128)(2,1)S(1)}, u32[]{:S(2)}, u32[]{:S(2)}) collective-permute-start(bf16[688,256]{1,0:T(8,128)(2,1)S(1)} %collective-permute-done.3.refs_4_), channel_id=1, source_target_pairs={{0,1},{1,0},{2,3},{3,2},{4,8},{5,9},{6,10},{7,11},{8,4},{9,5},{10,... | collective-permute-start | bytes 1056776 | tf_op jit(solution)/shard_map/ppermute | solution.py:128
  81.7 16.2 %collective-permute-start.17 = (bf16[688,256]{1,0:T(8,128)(2,1)S(1)}, bf16[688,256]{1,0:T(8,128)(2,1)S(1)}, u32[]{:S(2)}, u32[]{:S(2)}) collective-permute-start(bf16[688,256]{1,0:T(8,128)(2,1)S(1)} %collective-permute-done.14.refs_6_), channel_id=1, source_target_pairs={{0,16},{1,17},{2,18},{3,19},{4,5},{5,4},{6,7},{7,6},{8,9},{9,8},{1... | collective-permute-start | bytes 1056776 | tf_op jit(solution)/shard_map/ppermute | solution.py:132
  83.3 17.5 %collective-permute-start.10 = (bf16[688,256]{1,0:T(8,128)(2,1)S(1)}, bf16[688,256]{1,0:T(8,128)(2,1)S(1)}, u32[]{:S(2)}, u32[]{:S(2)}) collective-permute-start(bf16[688,256]{1,0:T(8,128)(2,1)S(1)} %collective-permute-done.9.refs_8_), channel_id=1, source_target_pairs={{0,4},{1,5},{2,6},{3,7},{4,0},{5,1},{6,2},{7,3},{8,12},{9,13},{10,... | collective-permute-start | bytes 1056776 | tf_op jit(solution)/shard_map/ppermute | solution.py:128
  91.7 16.5 %collective-permute-start.5 = (bf16[688,256]{1,0:T(8,128)(2,1)S(1)}, bf16[688,256]{1,0:T(8,128)(2,1)S(1)}, u32[]{:S(2)}, u32[]{:S(2)}) collective-permute-start(bf16[688,256]{1,0:T(8,128)(2,1)S(1)} %collective-permute-done.4.refs_4_), channel_id=1, source_target_pairs={{0,4},{1,5},{2,6},{3,7},{4,0},{5,1},{6,2},{7,3},{8,12},{9,13},{10,... | collective-permute-start | bytes 1056776 | tf_op jit(solution)/shard_map/ppermute | solution.py:128
  91.7 17.9 %collective-permute-start.22 = (bf16[688,256]{1,0:T(8,128)(2,1)S(1)}, bf16[688,256]{1,0:T(8,128)(2,1)S(1)}, u32[]{:S(2)}, u32[]{:S(2)}) collective-permute-start(bf16[688,256]{1,0:T(8,128)(2,1)S(1)} %collective-permute-done.19.refs_12_), channel_id=1, source_target_pairs={{0,16},{1,17},{2,18},{3,19},{4,5},{5,4},{6,7},{7,6},{8,9},{9,8},{1... | collective-permute-start | bytes 1056776 | tf_op jit(solution)/shard_map/ppermute | solution.py:132
  93.3 16.9 %collective-permute-start.11 = (bf16[688,256]{1,0:T(8,128)(2,1)S(1)}, bf16[688,256]{1,0:T(8,128)(2,1)S(1)}, u32[]{:S(2)}, u32[]{:S(2)}) collective-permute-start(bf16[688,256]{1,0:T(8,128)(2,1)S(1)} %collective-permute-done.9.refs_8_), channel_id=1, source_target_pairs={{0,1},{1,0},{2,3},{3,2},{4,20},{5,21},{6,22},{7,23},{8,24},{9,25},... | collective-permute-start | bytes 1056776 | tf_op jit(solution)/shard_map/ppermute | solution.py:132
  98.0 17.5 %collective-permute-start.6 = (bf16[688,256]{1,0:T(8,128)(2,1)S(1)}, bf16[688,256]{1,0:T(8,128)(2,1)S(1)}, u32[]{:S(2)}, u32[]{:S(2)}) collective-permute-start(bf16[688,256]{1,0:T(8,128)(2,1)S(1)} %collective-permute-done.4.refs_4_), channel_id=1, source_target_pairs={{0,1},{1,0},{2,3},{3,2},{4,20},{5,21},{6,22},{7,23},{8,24},{9,25},... | collective-permute-start | bytes 1056776 | tf_op jit(solution)/shard_map/ppermute | solution.py:132
  100.7 16.3 %collective-permute-start.12 = (bf16[688,256]{1,0:T(8,128)(2,1)S(1)}, bf16[688,256]{1,0:T(8,128)(2,1)S(1)}, u32[]{:S(2)}, u32[]{:S(2)}) collective-permute-start(bf16[688,256]{1,0:T(8,128)(2,1)S(1)} %collective-permute-done.10.refs_9_), channel_id=1, source_target_pairs={{0,16},{1,17},{2,18},{3,19},{4,5},{5,4},{6,7},{7,6},{8,9},{9,8},{1... | collective-permute-start | bytes 1056776 | tf_op jit(solution)/shard_map/ppermute | solution.py:132
  109.6 16.1 %collective-permute-start.37 = (bf16[688,128]{1,0:T(8,128)(2,1)S(1)}, bf16[688,128]{1,0:T(8,128)(2,1)S(1)}, u32[]{:S(2)}, u32[]{:S(2)}) collective-permute-start(bf16[688,128]{1,0:T(8,128)(2,1)S(1)} %collective-permute-done.29.refs_2_), channel_id=1, source_target_pairs={{0,16},{1,17},{2,18},{3,19},{4,5},{5,4},{6,7},{7,6},{8,9},{9,8},{1... | collective-permute-start | bytes 528392 | tf_op jit(solution)/shard_map/ppermute | solution.py:132
  110.1 18.9 %collective-permute-start.38 = (bf16[688,128]{1,0:T(8,128)(2,1)S(1)}, bf16[688,128]{1,0:T(8,128)(2,1)S(1)}, u32[]{:S(2)}, u32[]{:S(2)}) collective-permute-start(bf16[688,128]{1,0:T(8,128)(2,1)S(1)} %get-tuple-element.33), channel_id=1, source_target_pairs={{0,4},{1,5},{2,6},{3,7},{4,0},{5,1},{6,2},{7,3},{8,12},{9,13},{10,... | collective-permute-start | bytes 528392 | tf_op jit(solution)/shard_map/ppermute | solution.py:130
  128.9 15.0 %collective-permute-start.43 = (bf16[64,1024]{1,0:T(8,128)(2,1)S(1)}, bf16[64,1024]{1,0:T(8,128)(2,1)S(1)}, u32[]{:S(2)}, u32[]{:S(2)}) collective-permute-start(bf16[64,1024]{1,0:T(8,128)(2,1)S(1)} %get-tuple-element.35), channel_id=1, source_target_pairs={{0,1},{1,0},{2,3},{3,2},{4,5},{5,4},{6,7},{7,6},{8,9},{9,8},{10,11... | collective-permute-start | bytes 393224 | tf_op jit(solution)/shard_map/ppermute | solution.py:595
  (36 other events, 309.5 us)
where the time goes:
time: 149 us; the launch traced here: 148 us
  starting transfers between devices  79.4 us (53%)
  waiting for transfers between devices  55.7 us (37%)
  Pallas kernels  11.1 us (7%)
    ppermute x20, starting transfers between devices, line_exchange(): near[t, q] = lax.ppermute(operand, MESH, whole_moves(sizes, along))  50 us
    ppermute x20, waiting for transfers between devices, line_exchange(): near[t, q] = lax.ppermute(operand, MESH, whole_moves(sizes, along))  36.1 us
    ppermute x18, starting transfers between devices, line_exchange(): far[t, q] = lax.ppermute(near[t, q], MESH, whole_moves(sizes, across))  15.7 us
    ppermute x12, waiting for transfers between devices, over_tp(): lax.ppermute(blocks[d], 'tp', [(i, i ^ d) for i in range(n_tok)])  10.2 us
    ppermute x12, starting transfers between devices, over_tp(): lax.ppermute(blocks[d], 'tp', [(i, i ^ d) for i in range(n_tok)])  8.26 us
    ppermute x18, waiting for transfers between devices, line_exchange(): far[t, q] = lax.ppermute(near[t, q], MESH, whole_moves(sizes, across))  8.14 us
    ppermute x2, starting transfers between devices, line_exchange(): far[t, q] = lax.ppermute(halves[1], MESH, whole_moves(sizes, along))  5.43 us
    pallas_call x2, Pallas kernels, pair_part(): pl.pallas_call(functools.partial(pair_kernel, line, ks, own, n_tok), out_...  4.57 us
  transfers between devices with their start and end apart: 52, of which 18 were waited for; matrix products, arithmetic and copies ran while one was open for 0% of the time, Pallas kernels for 7%

commit v1 on v0

--- a/solution.py
+++ b/solution.py
@@ -11,6 +11,7 @@
 BF16 = jnp.bfloat16
 F32 = jnp.float32
 ANY = pl.BlockSpec(memory_space=pl.ANY)
+HBM = pl.BlockSpec(memory_space=pltpu.HBM)
 VMEM = pl.BlockSpec(memory_space=pltpu.VMEM)
 LANES = 128
 LONGEST_LINE = 8
@@ -169,7 +170,7 @@
     return pl.pallas_call(
         functools.partial(half_kernel, groups, cuts),
         out_shape=(jax.ShapeDtypeStruct((units, width), BF16),) * count,
-        in_specs=[ANY, VMEM][: len(operands)],
+        in_specs=[HBM if gain is None and count == 1 else ANY, VMEM][: len(operands)],
         out_specs=(VMEM,) * count,
         scratch_shapes=[
             pltpu.VMEM((count, units, width), F32),
@@ -425,65 +426,63 @@
         ref[:, start:stop] = part[d * rows:(d + 1) * rows]
 
 
-def down_own_kernel(form, blocks, n_tok, *refs):
-    count = len(form.sources(blocks))
-    (hidden_ref, master), some, (down_out,), parts, scratch = split(refs, 2, count, 1, n_tok)
-    held, wide, sem_in, sem_m, sem_out = scratch
-    mine = pltpu.make_async_copy(master, wide, sem_m)
+def place_own_kernel(form, master, down_out, own_ref, wide, sem):
+    mine = pltpu.make_async_copy(master, wide, sem.at[0])
     mine.start()
+    mine.wait()
+    own_ref[...] = wide[...].astype(BF16)
+    store = pltpu.make_async_copy(
+        own_ref, down_out.at[:, at(form.column((OWN,)), form.whole)], sem.at[1]
+    )
+    store.start()
+    store.wait()
+
+
+def place_own(form, master):
+    units = master.shape[0]
+    return pl.pallas_call(
+        functools.partial(place_own_kernel, form),
+        out_shape=(
+            jax.ShapeDtypeStruct((units, form.whole * form.line.count), BF16),
+            jax.ShapeDtypeStruct((units, form.whole), BF16),
+        ),
+        in_specs=[ANY],
+        out_specs=(ANY, VMEM),
+        scratch_shapes=[pltpu.VMEM((units, form.whole), F32), pltpu.SemaphoreType.DMA((2,))],
+        cost_estimate=cost(units * form.whole, 8 * units * form.whole),
+        compiler_params=pltpu.CompilerParams(vmem_limit_bytes=8 * 2**20),
+        name="place_own",
+    )(master)
+
+
+def down_part_kernel(form, blocks, n_tok, *refs):
+    mine = [n for n, block in enumerate(blocks) if block[0] == OWN]
+    (hidden_ref,), own, some, parts, (held, sem_in) = split(
+        refs, 1, len(mine), len(form.sources(blocks)), n_tok
+    )
+    loads = []
+    for n in mine:
+        start = form.widths(blocks[:n])
+        loads.append(
+            pltpu.make_async_copy(own[0], held.at[:, pl.ds(start, form.whole)], sem_in.at[n])
+        )
+    for load in loads:
+        load.start()
     waits = form.loads(blocks, some, held, sem_in)
-    first, *others = form.stores(blocks, held, down_out, sem_out)
-    mine.wait()
-    held[:, :form.whole] = wide[...].astype(BF16)
-    first.start()
-    multiply(hidden_ref, held, 0, form.whole, parts)
+    for load in loads:
+        load.wait()
     for wait in waits:
         wait()
-    for store in others:
-        store.start()
-    multiply(hidden_ref, held, form.whole, form.widths(blocks), parts)
-    for store in (first, *others):
-        store.wait()
-
-
-def down_own(form, blocks, n_tok, hidden, tables, master):
-    some = form.operands(blocks, tables)
-    units = master.shape[0]
-    rows = hidden.shape[0] // n_tok
-    width = form.widths(blocks)
-    return pl.pallas_call(
-        functools.partial(down_own_kernel, form, blocks, n_tok),
-        out_shape=(jax.ShapeDtypeStruct((units, form.whole * form.line.count), BF16),)
-        + (jax.ShapeDtypeStruct((rows, width), BF16),) * n_tok,
-        in_specs=[VMEM] + [ANY] * (len(some) + 1),
-        out_specs=(ANY,) + (VMEM,) * n_tok,
-        scratch_shapes=[
-            pltpu.VMEM((units, width), BF16),
-            pltpu.VMEM((units, form.whole), F32),
-            pltpu.SemaphoreType.DMA((len(blocks),)),
-            pltpu.SemaphoreType.DMA,
-            pltpu.SemaphoreType.DMA((len(blocks),)),
-        ],
-        cost_estimate=cost(2 * hidden.size * width, 4 * units * width),
-        compiler_params=pltpu.CompilerParams(vmem_limit_bytes=12 * 2**20),
-        name="down_own",
-    )(hidden, master, *some)
-
-
-def down_more_kernel(form, blocks, n_tok, *refs):
-    (hidden_ref,), some, parts, (held, sem_in) = split(refs, 1, len(form.sources(blocks)), n_tok)
-    for wait in form.loads(blocks, some, held, sem_in):
-        wait()
     multiply(hidden_ref, held, 0, form.widths(blocks), parts)
 
 
-def down_more(form, blocks, n_tok, hidden, tables):
-    some = form.operands(blocks, tables)
+def down_part(form, blocks, n_tok, hidden, tables, own=()):
+    some = [*own, *form.operands(blocks, tables)]
     units = hidden.shape[1]
     rows = hidden.shape[0] // n_tok
     width = form.widths(blocks)
     return pl.pallas_call(
-        functools.partial(down_more_kernel, form, blocks, n_tok),
+        functools.partial(down_part_kernel, form, blocks, n_tok),
         out_shape=(jax.ShapeDtypeStruct((rows, width), BF16),) * n_tok,
         in_specs=[VMEM] + [ANY] * len(some),
         out_specs=(VMEM,) * n_tok,
@@ -493,7 +492,7 @@
         ],
         cost_estimate=cost(2 * hidden.size * width, 2 * units * width),
         compiler_params=pltpu.CompilerParams(vmem_limit_bytes=8 * 2**20),
-        name="down_more",
+        name="down_part",
     )(hidden, *some)
 
 
@@ -634,13 +633,14 @@
         for block in ((k, s, n) for n in (0, 1) for k in range(last + 1) for s in (mine, other))
         if block not in early and block not in late
     )
-    down_ready, *own = down_own(form, early, n_tok, hidden, down_tables, down)
+    down_ready, piece = place_own(form, down)
+    own = down_part(form, early, n_tok, hidden, down_tables, [piece])
     own = over_tp(own, n_tok)
-    rest = down_more(form, between, n_tok, hidden, down_tables)
+    rest = down_part(form, between, n_tok, hidden, down_tables)
     rest = over_tp(rest, n_tok)
-    end = down_more(form, late, n_tok, hidden, down_tables)
+    end = down_part(form, late, n_tok, hidden, down_tables)
     end = over_tp(end, n_tok)
-    down_ready = place(form, between + late, down_ready, down_tables)
+    down_ready = place(form, early[1:] + between + late, down_ready, down_tables)
     head = mix(form, (early, between), tokens, (own, rest))
     result = finish_all(
         form, early + between, late, tokens,

time: 149 us -> 149 us (level)
    pallas_call x3 -> x4, Pallas kernels: 2.87 us -> 3.22 us  [the longest x3 2.07 us: down_part(): pl.pallas_call(functools.partial(down_part_kernel, form, blocks, n_tok),...]
  transfers between devices with their start and end apart: 52 -> 52, of which waited for: 18 -> 17; matrix products, arithmetic and copies ran while one was open for 0% -> 0% of each run, Pallas kernels for 7% -> 7%
where the time goes in v1:
time: 149 us
  starting transfers between devices  79.4 us (53%)
  waiting for transfers between devices  54.8 us (37%)
  Pallas kernels  11.8 us (8%)
  local copies, waits for them, and re-layouts  1.86 us (1%)
    ppermute x20, starting transfers between devices, line_exchange(): near[t, q] = lax.ppermute(operand, MESH, whole_moves(sizes, along))  50 us
    ppermute x20, waiting for transfers between devices, line_exchange(): near[t, q] = lax.ppermute(operand, MESH, whole_moves(sizes, along))  36.1 us
    ppermute x18, starting transfers between devices, line_exchange(): far[t, q] = lax.ppermute(near[t, q], MESH, whole_moves(sizes, across))  15.7 us
    ppermute x12, waiting for transfers between devices, over_tp(): lax.ppermute(blocks[d], 'tp', [(i, i ^ d) for i in range(n_tok)])  9.86 us
    ppermute x12, starting transfers between devices, over_tp(): lax.ppermute(blocks[d], 'tp', [(i, i ^ d) for i in range(n_tok)])  8.27 us
    ppermute x18, waiting for transfers between devices, line_exchange(): far[t, q] = lax.ppermute(near[t, q], MESH, whole_moves(sizes, across))  7.58 us
    ppermute x2, starting transfers between devices, line_exchange(): far[t, q] = lax.ppermute(halves[1], MESH, whole_moves(sizes, along))  5.43 us
    pallas_call x2, Pallas kernels, pair_part(): pl.pallas_call(functools.partial(pair_kernel, line, ks, own, n_tok), out_...  4.57 us
  transfers between devices with their start and end apart: 52, of which 17 were waited for; matrix products, arithmetic and copies ran while one was open for 0% of the time, Pallas kernels for 7%

profile of v1, /device:TPU:0, one launch (start us, length us, event | category | flops | bytes accessed | tf_op | source)
XLA Modules:
  0.0 148.8 jit_solution(15879302216129712641)
XLA Ops:
  2.2 3.1 %collective-permute-start.28 = (bf16[688,128]{1,0:T(8,128)(2,1)S(1)}, bf16[688,128]{1,0:T(8,128)(2,1)S(1)}, u32[]{:S(2)}, u32[]{:S(2)}) collective-permute-start(bf16[688,128]{1,0:T(8,128)(2,1)S(1)} %get-tuple-element.32), channel_id=1, source_target_pairs={{0,4},{1,5},{2,6},{3,7},{4,0},{5,1},{6,2},{7,3},{8,12},{9,13},{10,... | collective-permute-start | bytes 528392 | tf_op jit(solution)/shard_map/ppermute | solution.py:129
  5.4 3.2 %collective-permute-start.23 = (bf16[688,128]{1,0:T(8,128)(2,1)S(1)}, bf16[688,128]{1,0:T(8,128)(2,1)S(1)}, u32[]{:S(2)}, u32[]{:S(2)}) collective-permute-start(bf16[688,128]{1,0:T(8,128)(2,1)S(1)} %half_pieces.6), channel_id=1, source_target_pairs={{0,4},{1,5},{2,6},{3,7},{4,0},{5,1},{6,2},{7,3},{8,12},{9,13},{10,... | collective-permute-start | bytes 528392 | tf_op jit(solution)/shard_map/ppermute | solution.py:129
  9.5 4.0 %collective-permute-done.23.refs_1_.refs_2_ = bf16[688,128]{1,0:T(8,128)(2,1)S(1)} collective-permute-done((bf16[688,128]{1,0:T(8,128)(2,1)S(1)}, bf16[688,128]{1,0:T(8,128)(2,1)S(1)}, u32[]{:S(2)}, u32[]{:S(2)}) %collective-permute-start.23) | collective-permute-done | bytes 176160 | tf_op jit(solution)/shard_map/ppermute | solution.py:129
  13.5 1.7 %collective-permute-start.1 = (bf16[64,2048]{1,0:T(8,128)(2,1)S(1)}, bf16[64,2048]{1,0:T(8,128)(2,1)S(1)}, u32[]{:S(2)}, u32[]{:S(2)}) collective-permute-start(bf16[64,2048]{1,0:T(8,128)(2,1)S(1)} %norm_tokens.1.refs_0_), channel_id=1, source_target_pairs={{0,2},{1,3},{2,0},{3,1},{4,6},{5,7},{6,4},{7,5},{8,10},{9,11},{10,... | collective-permute-start | bytes 786440 | tf_op jit(solution)/shard_map/ppermute | solution.py:594
  17.6 15.3 %collective-permute-start.3 = (bf16[688,256]{1,0:T(8,128)(2,1)S(1)}, bf16[688,256]{1,0:T(8,128)(2,1)S(1)}, u32[]{:S(2)}, u32[]{:S(2)}) collective-permute-start(bf16[688,256]{1,0:T(8,128)(2,1)S(1)} %half_pieces.4), channel_id=1, source_target_pairs={{0,4},{1,5},{2,6},{3,7},{4,0},{5,1},{6,2},{7,3},{8,12},{9,13},{10,... | collective-permute-start | bytes 1056776 | tf_op jit(solution)/shard_map/ppermute | solution.py:129
  33.5 8.9 %collective-permute-start.30 = (bf16[688,128]{1,0:T(8,128)(2,1)S(1)}, bf16[688,128]{1,0:T(8,128)(2,1)S(1)}, u32[]{:S(2)}, u32[]{:S(2)}) collective-permute-start(bf16[688,128]{1,0:T(8,128)(2,1)S(1)} %collective-permute-done.29.refs_7_.refs_3_), channel_id=1, source_target_pairs={{0,4},{1,5},{2,6},{3,7},{4,0},{5,1},{6,2},{7,3},{8,12},{9,13},{10,... | collective-permute-start | bytes 528392 | tf_op jit(solution)/shard_map/ppermute | solution.py:129
  44.0 5.5 %collective-permute-done.8.refs_10_ = bf16[688,256]{1,0:T(8,128)(2,1)S(1)} collective-permute-done((bf16[688,256]{1,0:T(8,128)(2,1)S(1)}, bf16[688,256]{1,0:T(8,128)(2,1)S(1)}, u32[]{:S(2)}, u32[]{:S(2)}) %collective-permute-start.8) | collective-permute-done | bytes 352288 | tf_op jit(solution)/shard_map/ppermute | solution.py:129
  49.6 3.5 %collective-permute-start.27 = (bf16[688,128]{1,0:T(8,128)(2,1)S(1)}, bf16[688,128]{1,0:T(8,128)(2,1)S(1)}, u32[]{:S(2)}, u32[]{:S(2)}) collective-permute-start(bf16[688,128]{1,0:T(8,128)(2,1)S(1)} %collective-permute-done.26.refs_4_.refs_1_), channel_id=1, source_target_pairs={{0,4},{1,5},{2,6},{3,7},{4,0},{5,1},{6,2},{7,3},{8,12},{9,13},{10,... | collective-permute-start | bytes 528392 | tf_op jit(solution)/shard_map/ppermute | solution.py:129
  53.3 2.0 %collective-permute-start.32 = (bf16[688,128]{1,0:T(8,128)(2,1)S(1)}, bf16[688,128]{1,0:T(8,128)(2,1)S(1)}, u32[]{:S(2)}, u32[]{:S(2)}) collective-permute-start(bf16[688,128]{1,0:T(8,128)(2,1)S(1)} %collective-permute-done.31.refs_9_.refs_5_), channel_id=1, source_target_pairs={{0,4},{1,5},{2,6},{3,7},{4,0},{5,1},{6,2},{7,3},{8,12},{9,13},{10,... | collective-permute-start | bytes 528392 | tf_op jit(solution)/shard_map/ppermute | solution.py:129
  55.4 1.8 %collective-permute-done.25.refs_3_.refs_4_ = bf16[688,128]{1,0:T(8,128)(2,1)S(1)} collective-permute-done((bf16[688,128]{1,0:T(8,128)(2,1)S(1)}, bf16[688,128]{1,0:T(8,128)(2,1)S(1)}, u32[]{:S(2)}, u32[]{:S(2)}) %collective-permute-start.25) | collective-permute-done | bytes 176160 | tf_op jit(solution)/shard_map/ppermute | solution.py:129
  58.6 2.2 %collective-permute-done.27.refs_5_.refs_2_ = bf16[688,128]{1,0:T(8,128)(2,1)S(1)} collective-permute-done((bf16[688,128]{1,0:T(8,128)(2,1)S(1)}, bf16[688,128]{1,0:T(8,128)(2,1)S(1)}, u32[]{:S(2)}, u32[]{:S(2)}) %collective-permute-start.27) | collective-permute-done | bytes 176160 | tf_op jit(solution)/shard_map/ppermute | solution.py:129
  62.4 8.6 %collective-permute-done.32.refs_10_.refs_6_ = bf16[688,128]{1,0:T(8,128)(2,1)S(1)} collective-permute-done((bf16[688,128]{1,0:T(8,128)(2,1)S(1)}, bf16[688,128]{1,0:T(8,128)(2,1)S(1)}, u32[]{:S(2)}, u32[]{:S(2)}) %collective-permute-start.32) | collective-permute-done | bytes 176160 | tf_op jit(solution)/shard_map/ppermute | solution.py:129
  71.0 1.7 %collective-permute-start.19 = (bf16[688,256]{1,0:T(8,128)(2,1)S(1)}, bf16[688,256]{1,0:T(8,128)(2,1)S(1)}, u32[]{:S(2)}, u32[]{:S(2)}) collective-permute-start(bf16[688,256]{1,0:T(8,128)(2,1)S(1)} %collective-permute-done.18.refs_11_), channel_id=1, source_target_pairs={{0,4},{1,5},{2,6},{3,7},{4,0},{5,1},{6,2},{7,3},{8,12},{9,13},{10,... | collective-permute-start | bytes 1056776 | tf_op jit(solution)/shard_map/ppermute | solution.py:129
  74.8 5.2 %collective-permute-done.19.refs_12_ = bf16[688,256]{1,0:T(8,128)(2,1)S(1)} collective-permute-done((bf16[688,256]{1,0:T(8,128)(2,1)S(1)}, bf16[688,256]{1,0:T(8,128)(2,1)S(1)}, u32[]{:S(2)}, u32[]{:S(2)}) %collective-permute-start.19) | collective-permute-done | bytes 352288 | tf_op jit(solution)/shard_map/ppermute | solution.py:129
  83.3 8.4 %collective-permute-start.10 = (bf16[688,256]{1,0:T(8,128)(2,1)S(1)}, bf16[688,256]{1,0:T(8,128)(2,1)S(1)}, u32[]{:S(2)}, u32[]{:S(2)}) collective-permute-start(bf16[688,256]{1,0:T(8,128)(2,1)S(1)} %collective-permute-done.9.refs_8_), channel_id=1, source_target_pairs={{0,4},{1,5},{2,6},{3,7},{4,0},{5,1},{6,2},{7,3},{8,12},{9,13},{10,... | collective-permute-start | bytes 1056776 | tf_op jit(solution)/shard_map/ppermute | solution.py:129
  93.3 4.7 %collective-permute-done.17.refs_9_ = bf16[688,256]{1,0:T(8,128)(2,1)S(1)} collective-permute-done((bf16[688,256]{1,0:T(8,128)(2,1)S(1)}, bf16[688,256]{1,0:T(8,128)(2,1)S(1)}, u32[]{:S(2)}, u32[]{:S(2)}) %collective-permute-start.17) | collective-permute-done | bytes 352288 | tf_op jit(solution)/shard_map/ppermute | solution.py:133
  98.0 2.8 %collective-permute-done.10.refs_9_ = bf16[688,256]{1,0:T(8,128)(2,1)S(1)} collective-permute-done((bf16[688,256]{1,0:T(8,128)(2,1)S(1)}, bf16[688,256]{1,0:T(8,128)(2,1)S(1)}, u32[]{:S(2)}, u32[]{:S(2)}) %collective-permute-start.10) | collective-permute-done | bytes 352288 | tf_op jit(solution)/shard_map/ppermute | solution.py:129
  102.3 5.8 %collective-permute-done.5.refs_5_ = bf16[688,256]{1,0:T(8,128)(2,1)S(1)} collective-permute-done((bf16[688,256]{1,0:T(8,128)(2,1)S(1)}, bf16[688,256]{1,0:T(8,128)(2,1)S(1)}, u32[]{:S(2)}, u32[]{:S(2)}) %collective-permute-start.5) | collective-permute-done | bytes 352288 | tf_op jit(solution)/shard_map/ppermute | solution.py:129
  110.1 5.3 %collective-permute-start.38 = (bf16[688,128]{1,0:T(8,128)(2,1)S(1)}, bf16[688,128]{1,0:T(8,128)(2,1)S(1)}, u32[]{:S(2)}, u32[]{:S(2)}) collective-permute-start(bf16[688,128]{1,0:T(8,128)(2,1)S(1)} %get-tuple-element.33), channel_id=1, source_target_pairs={{0,4},{1,5},{2,6},{3,7},{4,0},{5,1},{6,2},{7,3},{8,12},{9,13},{10,... | collective-permute-start | bytes 528392 | tf_op jit(solution)/shard_map/ppermute | solution.py:131
  117.0 2.6 %collective-permute-done.7.refs_7_ = bf16[688,256]{1,0:T(8,128)(2,1)S(1)} collective-permute-done((bf16[688,256]{1,0:T(8,128)(2,1)S(1)}, bf16[688,256]{1,0:T(8,128)(2,1)S(1)}, u32[]{:S(2)}, u32[]{:S(2)}) %collective-permute-start.7) | collective-permute-done | bytes 352288 | tf_op jit(solution)/shard_map/ppermute | solution.py:133
  121.1 3.2 %pair_first.1 = (bf16[688,2048]{1,0:T(8,128)(2,1)}, bf16[688,2048]{1,0:T(8,128)(2,1)}, f32[2,256,688]{2,1,0:T(8,128)S(1)}) custom-call(bf16[64,2048]{1,0:T(8,128)(2,1)S(1)} %norm_tokens.1.refs_0_, bf16[64,2048]{1,0:T(8,128)(2,1)S(1)} %collective-permute-done.refs_1_, bf16[64,2048]{1,0:T(8,128)(2,1)S(1)} %collective-permute-done.1.refs_2_, ...), custom_call_target="tpu_custom_call" | custom-call | flops 1082130432 | bytes 10567680 | tf_op jit(solution)/shard_map/pair_first/pallas_call | solution.py:339
  129.3 2.6 %collective-permute-start.47 = (bf16[64,768]{1,0:T(8,128)(2,1)S(1)}, bf16[64,768]{1,0:T(8,128)(2,1)S(1)}, u32[]{:S(2)}, u32[]{:S(2)}) collective-permute-start(bf16[64,768]{1,0:T(8,128)(2,1)S(1)} %get-tuple-element.42), channel_id=1, source_target_pairs={{0,2},{1,3},{2,0},{3,1},{4,6},{5,7},{6,4},{7,5},{8,10},{9,11},{10,... | collective-permute-start | bytes 294920 | tf_op jit(solution)/shard_map/ppermute | solution.py:594
  135.5 7.2 %collective-permute-done.48.refs_8_ = bf16[64,768]{1,0:T(8,128)(2,1)S(1)} collective-permute-done((bf16[64,768]{1,0:T(8,128)(2,1)S(1)}, bf16[64,768]{1,0:T(8,128)(2,1)S(1)}, u32[]{:S(2)}, u32[]{:S(2)}) %collective-permute-start.48) | collective-permute-done | bytes 98336 | tf_op jit(solution)/shard_map/ppermute | solution.py:594
  144.2 2.0 %place.1 = bf16[688,2048]{1,0:T(8,128)(2,1)} custom-call(bf16[688,2048]{1,0:T(8,128)(2,1)} %get-tuple-element.31.refs_0_, bf16[688,128]{1,0:T(8,128)(2,1)S(1)} %collective-permute-done.23.refs_1_.refs_2_, bf16[688,128]{1,0:T(8,128)(2,1)S(1)} %collective-permute-done.24.refs_2_.refs_3_, ...), custom_call_target="tpu_custom_call", output_to_operand_aliasing={{}: (0, {})} | custom-call | bytes 4227072 | tf_op jit(solution)/shard_map/place/pallas_call | solution.py:514
  (110 shorter events, 36.5 us)
Async XLA Ops:
  13.5 19.4 %collective-permute-start.1 = (bf16[64,2048]{1,0:T(8,128)(2,1)S(1)}, bf16[64,2048]{1,0:T(8,128)(2,1)S(1)}, u32[]{:S(2)}, u32[]{:S(2)}) collective-permute-start(bf16[64,2048]{1,0:T(8,128)(2,1)S(1)} %norm_tokens.1.refs_0_), channel_id=1, source_target_pairs={{0,2},{1,3},{2,0},{3,1},{4,6},{5,7},{6,4},{7,5},{8,10},{9,11},{10,... | collective-permute-start | bytes 786440 | tf_op jit(solution)/shard_map/ppermute | solution.py:594
  15.2 17.8 %collective-permute-start.2 = (bf16[64,2048]{1,0:T(8,128)(2,1)S(1)}, bf16[64,2048]{1,0:T(8,128)(2,1)S(1)}, u32[]{:S(2)}, u32[]{:S(2)}) collective-permute-start(bf16[64,2048]{1,0:T(8,128)(2,1)S(1)} %norm_tokens.1.refs_0_), channel_id=1, source_target_pairs={{0,3},{1,2},{2,1},{3,0},{4,7},{5,6},{6,5},{7,4},{8,11},{9,10},{10,... | collective-permute-start | bytes 786440 | tf_op jit(solution)/shard_map/ppermute | solution.py:594
  15.2 17.8 %collective-permute-start.13 = (bf16[688,256]{1,0:T(8,128)(2,1)S(1)}, bf16[688,256]{1,0:T(8,128)(2,1)S(1)}, u32[]{:S(2)}, u32[]{:S(2)}) collective-permute-start(bf16[688,256]{1,0:T(8,128)(2,1)S(1)} %half_pieces.4), channel_id=1, source_target_pairs={{0,1},{1,0},{2,3},{3,2},{4,8},{5,9},{6,10},{7,11},{8,4},{9,5},{10,... | collective-permute-start | bytes 1056776 | tf_op jit(solution)/shard_map/ppermute | solution.py:129
  17.2 16.3 %collective-permute-start.18 = (bf16[688,256]{1,0:T(8,128)(2,1)S(1)}, bf16[688,256]{1,0:T(8,128)(2,1)S(1)}, u32[]{:S(2)}, u32[]{:S(2)}) collective-permute-start(bf16[688,256]{1,0:T(8,128)(2,1)S(1)} %half_pieces.5), channel_id=1, source_target_pairs={{0,1},{1,0},{2,3},{3,2},{4,8},{5,9},{6,10},{7,11},{8,4},{9,5},{10,... | collective-permute-start | bytes 1056776 | tf_op jit(solution)/shard_map/ppermute | solution.py:129
  17.6 24.8 %collective-permute-start.3 = (bf16[688,256]{1,0:T(8,128)(2,1)S(1)}, bf16[688,256]{1,0:T(8,128)(2,1)S(1)}, u32[]{:S(2)}, u32[]{:S(2)}) collective-permute-start(bf16[688,256]{1,0:T(8,128)(2,1)S(1)} %half_pieces.4), channel_id=1, source_target_pairs={{0,4},{1,5},{2,6},{3,7},{4,0},{5,1},{6,2},{7,3},{8,12},{9,13},{10,... | collective-permute-start | bytes 1056776 | tf_op jit(solution)/shard_map/ppermute | solution.py:129
  32.9 16.6 %collective-permute-start.8 = (bf16[688,256]{1,0:T(8,128)(2,1)S(1)}, bf16[688,256]{1,0:T(8,128)(2,1)S(1)}, u32[]{:S(2)}, u32[]{:S(2)}) collective-permute-start(bf16[688,256]{1,0:T(8,128)(2,1)S(1)} %half_pieces.5), channel_id=1, source_target_pairs={{0,4},{1,5},{2,6},{3,7},{4,0},{5,1},{6,2},{7,3},{8,12},{9,13},{10,... | collective-permute-start | bytes 1056776 | tf_op jit(solution)/shard_map/ppermute | solution.py:129
  33.0 16.6 %collective-permute-start.26 = (bf16[688,128]{1,0:T(8,128)(2,1)S(1)}, bf16[688,128]{1,0:T(8,128)(2,1)S(1)}, u32[]{:S(2)}, u32[]{:S(2)}) collective-permute-start(bf16[688,128]{1,0:T(8,128)(2,1)S(1)} %collective-permute-done.23.refs_1_.refs_2_), channel_id=1, source_target_pairs={{0,1},{1,0},{2,3},{3,2},{4,8},{5,9},{6,10},{7,11},{8,4},{9,5},{10,... | collective-permute-start | bytes 528392 | tf_op jit(solution)/shard_map/ppermute | solution.py:129
  33.0 20.1 %collective-permute-start.31 = (bf16[688,128]{1,0:T(8,128)(2,1)S(1)}, bf16[688,128]{1,0:T(8,128)(2,1)S(1)}, u32[]{:S(2)}, u32[]{:S(2)}) collective-permute-start(bf16[688,128]{1,0:T(8,128)(2,1)S(1)} %collective-permute-done.28.refs_6_.refs_5_), channel_id=1, source_target_pairs={{0,1},{1,0},{2,3},{3,2},{4,8},{5,9},{6,10},{7,11},{8,4},{9,5},{10,... | collective-permute-start | bytes 528392 | tf_op jit(solution)/shard_map/ppermute | solution.py:129
  33.5 19.8 %collective-permute-start.30 = (bf16[688,128]{1,0:T(8,128)(2,1)S(1)}, bf16[688,128]{1,0:T(8,128)(2,1)S(1)}, u32[]{:S(2)}, u32[]{:S(2)}) collective-permute-start(bf16[688,128]{1,0:T(8,128)(2,1)S(1)} %collective-permute-done.29.refs_7_.refs_3_), channel_id=1, source_target_pairs={{0,4},{1,5},{2,6},{3,7},{4,0},{5,1},{6,2},{7,3},{8,12},{9,13},{10,... | collective-permute-start | bytes 528392 | tf_op jit(solution)/shard_map/ppermute | solution.py:129
  53.1 21.6 %collective-permute-start.14 = (bf16[688,256]{1,0:T(8,128)(2,1)S(1)}, bf16[688,256]{1,0:T(8,128)(2,1)S(1)}, u32[]{:S(2)}, u32[]{:S(2)}) collective-permute-start(bf16[688,256]{1,0:T(8,128)(2,1)S(1)} %collective-permute-done.13.refs_5_), channel_id=1, source_target_pairs={{0,4},{1,5},{2,6},{3,7},{4,0},{5,1},{6,2},{7,3},{8,12},{9,13},{10,... | collective-permute-start | bytes 1056776 | tf_op jit(solution)/shard_map/ppermute | solution.py:129
  53.3 17.6 %collective-permute-start.32 = (bf16[688,128]{1,0:T(8,128)(2,1)S(1)}, bf16[688,128]{1,0:T(8,128)(2,1)S(1)}, u32[]{:S(2)}, u32[]{:S(2)}) collective-permute-start(bf16[688,128]{1,0:T(8,128)(2,1)S(1)} %collective-permute-done.31.refs_9_.refs_5_), channel_id=1, source_target_pairs={{0,4},{1,5},{2,6},{3,7},{4,0},{5,1},{6,2},{7,3},{8,12},{9,13},{10,... | collective-permute-start | bytes 528392 | tf_op jit(solution)/shard_map/ppermute | solution.py:129
  57.1 15.6 %collective-permute-start.36 = (bf16[688,128]{1,0:T(8,128)(2,1)S(1)}, bf16[688,128]{1,0:T(8,128)(2,1)S(1)}, u32[]{:S(2)}, u32[]{:S(2)}) collective-permute-start(bf16[688,128]{1,0:T(8,128)(2,1)S(1)} %collective-permute-done.26.refs_4_.refs_1_), channel_id=1, source_target_pairs={{0,1},{1,0},{2,3},{3,2},{4,20},{5,21},{6,22},{7,23},{8,24},{9,25},... | collective-permute-start | bytes 528392 | tf_op jit(solution)/shard_map/ppermute | solution.py:133
  57.1 17.1 %collective-permute-start.40 = (bf16[688,128]{1,0:T(8,128)(2,1)S(1)}, bf16[688,128]{1,0:T(8,128)(2,1)S(1)}, u32[]{:S(2)}, u32[]{:S(2)}) collective-permute-start(bf16[688,128]{1,0:T(8,128)(2,1)S(1)} %collective-permute-done.30.refs_8_.refs_4_), channel_id=1, source_target_pairs={{0,16},{1,17},{2,18},{3,19},{4,5},{5,4},{6,7},{7,6},{8,9},{9,8},{1... | collective-permute-start | bytes 528392 | tf_op jit(solution)/shard_map/ppermute | solution.py:133
  74.7 16.9 %collective-permute-start.4 = (bf16[688,256]{1,0:T(8,128)(2,1)S(1)}, bf16[688,256]{1,0:T(8,128)(2,1)S(1)}, u32[]{:S(2)}, u32[]{:S(2)}) collective-permute-start(bf16[688,256]{1,0:T(8,128)(2,1)S(1)} %collective-permute-done.3.refs_4_), channel_id=1, source_target_pairs={{0,1},{1,0},{2,3},{3,2},{4,8},{5,9},{6,10},{7,11},{8,4},{9,5},{10,... | collective-permute-start | bytes 1056776 | tf_op jit(solution)/shard_map/ppermute | solution.py:129
  81.7 16.2 %collective-permute-start.17 = (bf16[688,256]{1,0:T(8,128)(2,1)S(1)}, bf16[688,256]{1,0:T(8,128)(2,1)S(1)}, u32[]{:S(2)}, u32[]{:S(2)}) collective-permute-start(bf16[688,256]{1,0:T(8,128)(2,1)S(1)} %collective-permute-done.14.refs_6_), channel_id=1, source_target_pairs={{0,16},{1,17},{2,18},{3,19},{4,5},{5,4},{6,7},{7,6},{8,9},{9,8},{1... | collective-permute-start | bytes 1056776 | tf_op jit(solution)/shard_map/ppermute | solution.py:133
  83.3 17.5 %collective-permute-start.10 = (bf16[688,256]{1,0:T(8,128)(2,1)S(1)}, bf16[688,256]{1,0:T(8,128)(2,1)S(1)}, u32[]{:S(2)}, u32[]{:S(2)}) collective-permute-start(bf16[688,256]{1,0:T(8,128)(2,1)S(1)} %collective-permute-done.9.refs_8_), channel_id=1, source_target_pairs={{0,4},{1,5},{2,6},{3,7},{4,0},{5,1},{6,2},{7,3},{8,12},{9,13},{10,... | collective-permute-start | bytes 1056776 | tf_op jit(solution)/shard_map/ppermute | solution.py:129
  91.7 16.5 %collective-permute-start.5 = (bf16[688,256]{1,0:T(8,128)(2,1)S(1)}, bf16[688,256]{1,0:T(8,128)(2,1)S(1)}, u32[]{:S(2)}, u32[]{:S(2)}) collective-permute-start(bf16[688,256]{1,0:T(8,128)(2,1)S(1)} %collective-permute-done.4.refs_4_), channel_id=1, source_target_pairs={{0,4},{1,5},{2,6},{3,7},{4,0},{5,1},{6,2},{7,3},{8,12},{9,13},{10,... | collective-permute-start | bytes 1056776 | tf_op jit(solution)/shard_map/ppermute | solution.py:129
  91.7 17.9 %collective-permute-start.22 = (bf16[688,256]{1,0:T(8,128)(2,1)S(1)}, bf16[688,256]{1,0:T(8,128)(2,1)S(1)}, u32[]{:S(2)}, u32[]{:S(2)}) collective-permute-start(bf16[688,256]{1,0:T(8,128)(2,1)S(1)} %collective-permute-done.19.refs_12_), channel_id=1, source_target_pairs={{0,16},{1,17},{2,18},{3,19},{4,5},{5,4},{6,7},{7,6},{8,9},{9,8},{1... | collective-permute-start | bytes 1056776 | tf_op jit(solution)/shard_map/ppermute | solution.py:133
  93.3 16.9 %collective-permute-start.11 = (bf16[688,256]{1,0:T(8,128)(2,1)S(1)}, bf16[688,256]{1,0:T(8,128)(2,1)S(1)}, u32[]{:S(2)}, u32[]{:S(2)}) collective-permute-start(bf16[688,256]{1,0:T(8,128)(2,1)S(1)} %collective-permute-done.9.refs_8_), channel_id=1, source_target_pairs={{0,1},{1,0},{2,3},{3,2},{4,20},{5,21},{6,22},{7,23},{8,24},{9,25},... | collective-permute-start | bytes 1056776 | tf_op jit(solution)/shard_map/ppermute | solution.py:133
  98.0 17.5 %collective-permute-start.6 = (bf16[688,256]{1,0:T(8,128)(2,1)S(1)}, bf16[688,256]{1,0:T(8,128)(2,1)S(1)}, u32[]{:S(2)}, u32[]{:S(2)}) collective-permute-start(bf16[688,256]{1,0:T(8,128)(2,1)S(1)} %collective-permute-done.4.refs_4_), channel_id=1, source_target_pairs={{0,1},{1,0},{2,3},{3,2},{4,20},{5,21},{6,22},{7,23},{8,24},{9,25},... | collective-permute-start | bytes 1056776 | tf_op jit(solution)/shard_map/ppermute | solution.py:133
  100.7 16.3 %collective-permute-start.12 = (bf16[688,256]{1,0:T(8,128)(2,1)S(1)}, bf16[688,256]{1,0:T(8,128)(2,1)S(1)}, u32[]{:S(2)}, u32[]{:S(2)}) collective-permute-start(bf16[688,256]{1,0:T(8,128)(2,1)S(1)} %collective-permute-done.10.refs_9_), channel_id=1, source_target_pairs={{0,16},{1,17},{2,18},{3,19},{4,5},{5,4},{6,7},{7,6},{8,9},{9,8},{1... | collective-permute-start | bytes 1056776 | tf_op jit(solution)/shard_map/ppermute | solution.py:133
  109.6 16.1 %collective-permute-start.37 = (bf16[688,128]{1,0:T(8,128)(2,1)S(1)}, bf16[688,128]{1,0:T(8,128)(2,1)S(1)}, u32[]{:S(2)}, u32[]{:S(2)}) collective-permute-start(bf16[688,128]{1,0:T(8,128)(2,1)S(1)} %collective-permute-done.27.refs_5_.refs_2_), channel_id=1, source_target_pairs={{0,16},{1,17},{2,18},{3,19},{4,5},{5,4},{6,7},{7,6},{8,9},{9,8},{1... | collective-permute-start | bytes 528392 | tf_op jit(solution)/shard_map/ppermute | solution.py:133
  110.1 19.2 %collective-permute-start.38 = (bf16[688,128]{1,0:T(8,128)(2,1)S(1)}, bf16[688,128]{1,0:T(8,128)(2,1)S(1)}, u32[]{:S(2)}, u32[]{:S(2)}) collective-permute-start(bf16[688,128]{1,0:T(8,128)(2,1)S(1)} %get-tuple-element.33), channel_id=1, source_target_pairs={{0,4},{1,5},{2,6},{3,7},{4,0},{5,1},{6,2},{7,3},{8,12},{9,13},{10,... | collective-permute-start | bytes 528392 | tf_op jit(solution)/shard_map/ppermute | solution.py:131
  129.2 15.0 %collective-permute-start.43 = (bf16[64,1024]{1,0:T(8,128)(2,1)S(1)}, bf16[64,1024]{1,0:T(8,128)(2,1)S(1)}, u32[]{:S(2)}, u32[]{:S(2)}) collective-permute-start(bf16[64,1024]{1,0:T(8,128)(2,1)S(1)} %get-tuple-element.37), channel_id=1, source_target_pairs={{0,1},{1,0},{2,3},{3,2},{4,5},{5,4},{6,7},{7,6},{8,9},{9,8},{10,11... | collective-permute-start | bytes 393224 | tf_op jit(solution)/shard_map/ppermute | solution.py:594
  (36 other events, 310.7 us)
